TPU v7x, 32 devices: a whole 2x2x4 slice. The times are simulated.
32 devices in a mesh: grp: 2 (over y), fs: 4 (over z), tp: 4 (over x, core).
Axes of the slice: x: 2, y: 2, z: 4, core: 2. Of those that a mesh axis runs over, the one named last changes fastest.
Arguments:
- tokens: bfloat16 [1792, 2048], P(('grp', 'fs'), 'tp'), parts along dimension 0, may hold values from -6 to 6
- route_ids: int32 [1792, 2], P(('grp', 'fs')), parts along dimension 0, may hold values from 0 to 3, all different within a row; in each aligned block of 224 rows (0 to 223, 224 to 447, ...) at most 168 rows name the same one
- route_weights: float32 [1792, 2], P(('grp', 'fs')), parts along dimension 0, may hold values from 0.25 to 1
- norm_gain: float32 [2048], P('fs'), may hold values from 0.1 to 1.9
- gate_master: float32 [4, 2048, 512], P(None, 'fs', 'tp'), may hold values from -0.125 to 0.125
- up_master: float32 [4, 2048, 512], P(None, 'fs', 'tp'), may hold values from -0.125 to 0.125
- down_master: float32 [4, 2048, 512], P(None, 'fs', 'tp'), may hold values from -0.25 to 0.25
Outputs:
- gate_serve: bfloat16 [8, 2048, 512], P(('grp', 'fs'), None, 'tp'), parts along dimension 0
- up_serve: bfloat16 [8, 2048, 512], P(('grp', 'fs'), None, 'tp'), parts along dimension 0
- down_serve: bfloat16 [8, 2048, 512], P(('grp', 'fs'), None, 'tp'), parts along dimension 0
- moe_output: bfloat16 [1792, 2048], P(('grp', 'fs'), 'tp'), parts along dimension 0
There are 2 independent parts, one for each index of `grp`. A program takes and returns all parts, laid end to end along the dimension named above; an argument that names none is the same for every part. Nothing has to cross between parts.
Inputs may be any that keep to these rules, and one draw needn't show every extreme that they name: `route_ids`: the 2 experts of a row differ; within the rows of one index of fs (aligned blocks of 224 rows) no expert is named more than 168 times.
All inputs are finite; a program needn't handle non-finite values.
Results may differ from a plain program's by a relative error of at most 0.012.
Values may be sent and summed in bfloat16 or wider, within the bound.
A program may use at most 64 MiB of HBM per device.

v0:
```python
import jax
import jax.numpy as jnp
from jax import lax
from jax.sharding import PartitionSpec as P

norm_epsilon = 1e-06


def slot_numbers(route_ids, experts, capacity):
    flat_ids = route_ids.reshape(-1)
    onehot = (flat_ids[:, None] == jnp.arange(experts, dtype=jnp.int32)[None, :]).astype(jnp.int32)
    before = jnp.cumsum(onehot, axis=0) - onehot
    position = jnp.sum(before * onehot, axis=1)
    return (flat_ids * capacity + position).reshape(route_ids.shape)


def local(tokens, route_ids, route_weights, norm_gain, gate_master, up_master, down_master):
    experts = gate_master.shape[0]
    shards = lax.axis_size("fs")
    columns = lax.axis_size("tp")
    per_device = experts // shards
    tok_rows = route_ids.shape[0]
    top_count = route_ids.shape[1]
    local_width = tokens.shape[1]
    model_width = local_width * columns
    capacity = max(2, 3 * tok_rows * top_count // (2 * experts))
    row_gain = norm_gain[None, :, None]
    gate_half = (gate_master * row_gain).astype(jnp.bfloat16)
    up_half = (up_master * row_gain).astype(jnp.bfloat16)
    down_half = down_master.astype(jnp.bfloat16)
    gate_serve, up_serve, down_serve = (
        lax.all_to_all(gate_half, "fs", split_axis=0, concat_axis=1, tiled=True),
        lax.all_to_all(up_half, "fs", split_axis=0, concat_axis=1, tiled=True),
        lax.all_to_all(down_half, "fs", split_axis=0, concat_axis=1, tiled=True),
    )
    slot_ids = slot_numbers(route_ids, experts, capacity)
    slot_range = jnp.arange(experts * capacity, dtype=jnp.int32)
    selects = [
        (slot_ids[:, rank_slot, None] == slot_range[None, :]).astype(jnp.bfloat16)
        for rank_slot in range(top_count)
    ]
    placing = selects[0]
    for extra in selects[1:]:
        placing = placing + extra
    local_values = tokens.astype(jnp.float32)
    squares = lax.psum(jnp.sum(local_values * local_values, axis=1), "tp")
    inverse = lax.rsqrt(squares / model_width + norm_epsilon)[:, None]
    normed = (local_values * inverse).astype(jnp.bfloat16)
    buffer = jnp.einsum("ts,td->sd", placing, normed, preferred_element_type=jnp.float32).astype(
        jnp.bfloat16
    )
    arrived = lax.all_to_all(
        buffer.reshape(shards, per_device * capacity, local_width),
        "fs",
        split_axis=0,
        concat_axis=0,
        tiled=True,
    )
    arrived = arrived.reshape(shards, per_device, capacity, local_width)
    partial_value = lax.all_gather(arrived, "tp", axis=3, tiled=True)
    gate_sum = jnp.einsum(
        "sxcd,xdf->xscf", partial_value, gate_serve, preferred_element_type=jnp.float32
    )
    up_sum = jnp.einsum(
        "sxcd,xdf->xscf", partial_value, up_serve, preferred_element_type=jnp.float32
    )
    hidden = (jax.nn.silu(gate_sum) * up_sum).astype(jnp.bfloat16)
    products = jnp.einsum("xdf,xscf->dsxc", down_serve, hidden, preferred_element_type=jnp.float32)
    summed = lax.psum_scatter(
        products.reshape(local_width * lax.axis_size("tp"), shards * per_device * capacity).astype(
            jnp.bfloat16
        ),
        "tp",
        scatter_dimension=0,
        tiled=True,
    )
    returned = lax.all_to_all(
        summed.reshape(local_width, shards, per_device * capacity),
        "fs",
        split_axis=1,
        concat_axis=1,
        tiled=True,
    )
    returned = returned.reshape(local_width, experts * capacity)
    combined = jnp.zeros((tok_rows, local_width), jnp.float32)
    for rank_slot in range(top_count):
        picked = jnp.einsum(
            "ts,ds->td", selects[rank_slot], returned, preferred_element_type=jnp.float32
        )
        combined = combined + route_weights[:, rank_slot : rank_slot + 1] * picked
    return (gate_serve, up_serve, down_serve, combined.astype(jnp.bfloat16))


def solution(mesh):
    placed = (
        P(("grp", "fs"), "tp"),
        P(("grp", "fs"), None),
        P(("grp", "fs"), None),
        P("fs"),
        P(None, "fs", "tp"),
        P(None, "fs", "tp"),
        P(None, "fs", "tp"),
    )
    return jax.shard_map(
        local,
        mesh=mesh,
        in_specs=placed,
        out_specs=(
            P(("grp", "fs"), None, "tp"),
            P(("grp", "fs"), None, "tp"),
            P(("grp", "fs"), None, "tp"),
            P(("grp", "fs"), "tp"),
        ),
        check_vma=False,
    )
```

profile of v0, /device:TPU:0, one launch (start us, length us, event | category | flops | bytes accessed | tf_op | source)
XLA Modules:
  0.0 170.7 jit_solution(8881094231520576288)
XLA Ops:
  7.2 0.9 copy.17
  8.4 1.2 reduce-window.6
  10.3 0.7 multiply_add_fusion
  11.0 1.1 fusion.5
  12.1 8.4 %psum.7 = f32[224]{0:T(256)S(1)} all-reduce(f32[224]{0:T(256)S(1)} %fusion.5), channel_id=1, replica_groups=mesh['grp'=2,'fs'=4,'tp'=4] {'tp'}, use_global_device_ids=true, to_apply=%region_4.5 | all-reduce | flops 224 | bytes 1792 | tf_op jit(solution)/shard_map/psum | solution.py:46
  20.5 1.5 convolution_convert_fusion.1
  22.0 21.6 %all_to_all.46 = bf16[4,168,512]{2,1,0:T(8,128)(2,1)} all-to-all(bf16[4,168,512]{2,1,0:T(8,128)(2,1)S(1)} %bitcast.48), channel_id=1, replica_groups=mesh['grp'=2,'fs'=4,'tp'=4] {'fs'}, dimensions={0} | all-to-all | bytes 1376256 | tf_op jit(solution)/shard_map/all_to_all | solution.py:52
  43.6 1.0 multiply_convert_fusion
  44.6 16.2 %all_to_all.47 = bf16[4,512,128]{2,1,0:T(8,128)(2,1)S(1)} all-to-all(bf16[4,512,128]{2,1,0:T(8,128)(2,1)S(1)} %get-tuple-element.9), channel_id=1, replica_groups=mesh['grp'=2,'fs'=4,'tp'=4] {'fs'}, dimensions={0} | all-to-all | bytes 1048576 | tf_op jit(solution)/shard_map/all_to_all | solution.py:32
  60.9 3.5 %all-to-all-start.1 = ((bf16[4,512,128]{2,1,0:T(8,128)(2,1)}), bf16[4,512,128]{2,1,0:T(8,128)(2,1)S(1)}, u32[]{:S(2)}, u32[]{:S(2)}) async-start(bf16[4,512,128]{2,1,0:T(8,128)(2,1)} %get-tuple-element.8), calls=%async_computation.1 | async-start | bytes 1048576 | tf_op jit(solution)/shard_map/all_to_all | solution.py:33
  64.4 0.9 convert_element_type.49
  65.2 12.6 %all-to-all-done.1 = bf16[4,512,128]{2,1,0:T(8,128)(2,1)S(1)} async-done(((bf16[4,512,128]{2,1,0:T(8,128)(2,1)}), bf16[4,512,128]{2,1,0:T(8,128)(2,1)S(1)}, u32[]{:S(2)}, u32[]{:S(2)}) %all-to-all-start.1) | async-done | bytes 524320 | tf_op jit(solution)/shard_map/all_to_all | solution.py:33
  77.9 4.1 %all-to-all-start.2 = ((bf16[4,512,128]{2,1,0:T(8,128)(2,1)}), bf16[4,512,128]{2,1,0:T(8,128)(2,1)}, u32[]{:S(2)}, u32[]{:S(2)}) async-start(bf16[4,512,128]{2,1,0:T(8,128)(2,1)} %convert_element_type.49), calls=%async_computation.2 | async-start | bytes 1048576 | tf_op jit(solution)/shard_map/all_to_all | solution.py:34
  82.1 3.5 %fusion.27 = f32[4,168,128]{2,1,0:T(8,128)} fusion(bf16[4,168,2048]{2,1,0:T(8,128)(2,1)} %all-gather.3.cloned.1.call-done, bf16[2048,128,1]{1,0,2:T(8,128)(2,1)S(1)} %bitcast.41), kind=kOutput, calls=%fused_computation.44 | convolution fusion | flops 352321536 | bytes 3620864 | tf_op jit(solution)/shard_map/sxcd,xdf->xscf/dot_general | solution.py:61
  85.7 10.5 %all-to-all-done.2 = bf16[4,512,128]{2,1,0:T(8,128)(2,1)} async-done(((bf16[4,512,128]{2,1,0:T(8,128)(2,1)}), bf16[4,512,128]{2,1,0:T(8,128)(2,1)}, u32[]{:S(2)}, u32[]{:S(2)}) %all-to-all-start.2) | async-done | bytes 524320 | tf_op jit(solution)/shard_map/all_to_all | solution.py:34
  96.1 5.8 %convolution_convert_fusion = bf16[4,168,2048]{2,1,0:T(8,128)(2,1)} fusion(bf16[2048,128,1]{1,0,2:T(8,128)(2,1)} %bitcast.13, bf16[4,168,2048]{2,1,0:T(8,128)(2,1)S(1)} %copy-done, bf16[2048,128,1]{1,0,2:T(8,128)(2,1)} %bitcast.43, f32[4,168,128]{2,1,0:T(8,128)} %fusion.27), kind=kOutput, calls=%fused_computation | convolution fusion | flops 706535424 | bytes 6897664 | tf_op jit(solution)/shard_map/xdf,xscf->dsxc/dot_general | solution.py:68
  102.0 34.5 %reduce-scatter.2.cloned.1.call-done = bf16[512,672]{0,1:T(8,128)(2,1)} async-done(((bf16[2048,672]{0,1:T(8,128)(2,1)}), bf16[512,672]{0,1:T(8,128)(2,1)}) %reduce-scatter.2.cloned.1.call-update) | async-done | bytes 688144 | tf_op jit(solution)/shard_map/reduce_scatter | solution.py:69
  136.5 4.6 %all-to-all-start.4 = ((bf16[512,4,168]{0,2,1:T(8,128)(2,1)}), bf16[512,4,168]{0,2,1:T(8,128)(2,1)S(1)}, u32[]{:S(2)}, u32[]{:S(2)}) async-start(bf16[512,4,168]{0,2,1:T(8,128)(2,1)} %bitcast.47), calls=%async_computation.5 | async-start | bytes 1376256 | tf_op jit(solution)/shard_map/all_to_all | solution.py:77
  141.1 17.8 %all-to-all-done.4 = bf16[512,4,168]{0,2,1:T(8,128)(2,1)S(1)} async-done(((bf16[512,4,168]{0,2,1:T(8,128)(2,1)}), bf16[512,4,168]{0,2,1:T(8,128)(2,1)S(1)}, u32[]{:S(2)}, u32[]{:S(2)}) %all-to-all-start.4) | async-done | bytes 688160 | tf_op jit(solution)/shard_map/all_to_all | solution.py:77
  158.9 0.4 convolution_multiply_fusion.1
  159.3 1.1 fusion.1
  160.4 0.8 copy.25
  161.2 0.8 copy.26
  162.0 1.9 %copy.27 = bf16[1,2048,128]{2,1,0:T(8,128)(2,1)} copy(bf16[1,2048,128]{2,1,0:T(8,128)(2,1)} %bitcast.2) | data formatting | bytes 1048576
  (35 shorter events, 1.1 us)
Async XLA Ops:
  7.2 36.4 %copy-start.7 = (f32[512]{0:T(512)S(1)}, f32[512]{0:T(512)}, u32[]{:S(2)}) copy-start(f32[512]{0:T(512)} %param.10) | copy-start | bytes 6148
  7.2 36.4 %copy-start.5 = (f32[4,512,128]{2,1,0:T(8,128)S(1)}, f32[4,512,128]{2,1,0:T(8,128)}, u32[]{:S(2)}) copy-start(f32[4,512,128]{2,1,0:T(8,128)} %param.11) | copy-start | bytes 3145732
  7.2 36.4 %copy-start.4 = (f32[4,512,128]{2,1,0:T(8,128)S(1)}, f32[4,512,128]{2,1,0:T(8,128)}, u32[]{:S(2)}) copy-start(f32[4,512,128]{2,1,0:T(8,128)} %param.12) | copy-start | bytes 3145732
  7.2 74.9 %all-gather.3.cloned.1.call-start = ((), (), s32[]{:S(2)}) async-start(), calls=%async_computation.7 | async-start | bytes 3440640 | tf_op jit(solution)/shard_map/all_gather | solution.py:60
  43.6 20.8 %copy-start.3 = (f32[4,512,128]{2,1,0:T(8,128)S(1)}, f32[4,512,128]{2,1,0:T(8,128)}, u32[]{:S(2)}) copy-start(f32[4,512,128]{2,1,0:T(8,128)} %param.13) | copy-start | bytes 3145732
  60.9 17.0 %all-to-all-start.1 = ((bf16[4,512,128]{2,1,0:T(8,128)(2,1)}), bf16[4,512,128]{2,1,0:T(8,128)(2,1)S(1)}, u32[]{:S(2)}, u32[]{:S(2)}) async-start(bf16[4,512,128]{2,1,0:T(8,128)(2,1)} %get-tuple-element.8), calls=%async_computation.1 | async-start | bytes 1048576 | tf_op jit(solution)/shard_map/all_to_all | solution.py:33
  77.9 4.2 %copy-start.1 = (bf16[4,512,128]{2,1,0:T(8,128)(2,1)}, bf16[4,512,128]{2,1,0:T(8,128)(2,1)S(1)}, u32[]{:S(2)}) copy-start(bf16[4,512,128]{2,1,0:T(8,128)(2,1)S(1)} %all-to-all-done.1) | copy-start | bytes 1572868
  77.9 18.3 %all-to-all-start.2 = ((bf16[4,512,128]{2,1,0:T(8,128)(2,1)}), bf16[4,512,128]{2,1,0:T(8,128)(2,1)}, u32[]{:S(2)}, u32[]{:S(2)}) async-start(bf16[4,512,128]{2,1,0:T(8,128)(2,1)} %convert_element_type.49), calls=%async_computation.2 | async-start | bytes 1048576 | tf_op jit(solution)/shard_map/all_to_all | solution.py:34
  82.0 54.5 %reduce-scatter.2.cloned.1.call-start = ((), (), s32[]{:S(2)}) async-start(), calls=%async_computation.6 | async-start | bytes 3440640 | tf_op jit(solution)/shard_map/reduce_scatter | solution.py:69
  82.1 14.0 %copy-start = (bf16[4,168,2048]{2,1,0:T(8,128)(2,1)S(1)}, bf16[4,168,2048]{2,1,0:T(8,128)(2,1)}, u32[]{:S(2)}) copy-start(bf16[4,168,2048]{2,1,0:T(8,128)(2,1)} %all-gather.3.cloned.1.call-done) | copy-start | bytes 8257540
  102.0 39.1 %copy-start.6 = (f32[224,2]{0,1:T(2,128)S(1)}, f32[224,2]{0,1:T(2,128)}, u32[]{:S(2)}) copy-start(f32[224,2]{0,1:T(2,128)} %param.9) | copy-start | bytes 5380
  102.0 59.2 %copy-start.2 = (bf16[4,512,128]{2,1,0:T(8,128)(2,1)S(1)}, bf16[4,512,128]{2,1,0:T(8,128)(2,1)}, u32[]{:S(2)}) copy-start(bf16[4,512,128]{2,1,0:T(8,128)(2,1)} %copy-done.1) | copy-start | bytes 1572868
  136.5 22.4 %all-to-all-start.4 = ((bf16[512,4,168]{0,2,1:T(8,128)(2,1)}), bf16[512,4,168]{0,2,1:T(8,128)(2,1)S(1)}, u32[]{:S(2)}, u32[]{:S(2)}) async-start(bf16[512,4,168]{0,2,1:T(8,128)(2,1)} %bitcast.47), calls=%async_computation.5 | async-start | bytes 1376256 | tf_op jit(solution)/shard_map/all_to_all | solution.py:77
Sparse Core Ops, SparseCore 0:
  43.7 25.4 all-gather.2
  102.1 34.3 reduce-scatter.1
where the time goes:
time: 171 us
  waiting for transfers between devices  75.5 us (44%)
  blocking collectives  46.2 us (27%)
  between operations  14.2 us (8%)
  starting transfers between devices  12.3 us (7%)
  matrix products  12.3 us (7%)
  other arithmetic  5.18 us (3%)
  local copies, waits for them, and re-layouts  5.04 us (3%)
    reduce_scatter x1, waiting for transfers between devices, local(): lax.psum_scatter(products.reshape(local_width * lax.axis_size('tp'), shar...  34.5 us
    all_to_all x1, blocking collectives, local(): lax.all_to_all(buffer.reshape(shards, per_device * capacity, local_width)...  21.6 us
    all_to_all x1, waiting for transfers between devices, local(): lax.all_to_all(summed.reshape(local_width, shards, per_device * capacity)...  17.8 us
    all_to_all x1, blocking collectives, local(): lax.all_to_all(gate_half, 'fs', split_axis=0, concat_axis=1, tiled=True)  16.2 us
    all_to_all x1, waiting for transfers between devices, local(): lax.all_to_all(up_half, 'fs', split_axis=0, concat_axis=1, tiled=True)  12.6 us
    all_to_all x1, waiting for transfers between devices, local(): lax.all_to_all(down_half, 'fs', split_axis=0, concat_axis=1, tiled=True)  10.5 us
    psum x1, blocking collectives, local(): squares = lax.psum(jnp.sum(local_values * local_values, axis=1), 'tp')  8.37 us
    dot_general x1, matrix products, local(): jnp.einsum('xdf,xscf->dsxc', down_serve, hidden, preferred_element_type=j...  5.82 us
  transfers between devices with their start and end apart: 5, of which 4 were waited for; matrix products, arithmetic and copies ran while one was open for 3% of the time, Pallas kernels for 0%

commit v1 on v0

--- a/solution.py
+++ b/solution.py
@@ -4,6 +4,29 @@
 from jax.sharding import PartitionSpec as P
 
 norm_epsilon = 1e-06
+
+
+def split_up(shard, dim, count):
+    before, after = (shard.shape[:dim], shard.shape[dim + 1 :])
+    return jnp.moveaxis(shard.reshape(*before, count, -1, *after), dim, 0)
+
+
+def joined_along(blocks, dim):
+    shape = list(blocks.shape[1:])
+    shape[dim] *= blocks.shape[0]
+    return jnp.moveaxis(blocks, 0, dim).reshape(shape)
+
+
+def rotated_exchange(x, axis, split_dim, concat_dim):
+    size, place = (lax.axis_size(axis), lax.axis_index(axis))
+    pieces = split_up(x, split_dim, size)
+    whole = pieces
+    for turn in range(1, size):
+        target, source = ((place + turn) % size, (place - turn) % size)
+        sent = lax.dynamic_index_in_dim(pieces, target, 0)
+        partner_block = lax.ppermute(sent, axis, [(i, (i + turn) % size) for i in range(size)])
+        whole = lax.dynamic_update_slice_in_dim(whole, partner_block, source, axis=0)
+    return joined_along(whole, concat_dim)
 
 
 def slot_numbers(route_ids, experts, capacity):
@@ -49,12 +72,8 @@
     buffer = jnp.einsum("ts,td->sd", placing, normed, preferred_element_type=jnp.float32).astype(
         jnp.bfloat16
     )
-    arrived = lax.all_to_all(
-        buffer.reshape(shards, per_device * capacity, local_width),
-        "fs",
-        split_axis=0,
-        concat_axis=0,
-        tiled=True,
+    arrived = rotated_exchange(
+        buffer.reshape(shards, per_device * capacity, local_width), "fs", 0, 0
     )
     arrived = arrived.reshape(shards, per_device, capacity, local_width)
     partial_value = lax.all_gather(arrived, "tp", axis=3, tiled=True)

time: 171 us -> 174 us (1.018)
  blocking collectives: 46.2 us -> 28.4 us
  waiting for transfers between devices: 75.5 us -> 89.7 us
  starting transfers between devices: 12.3 us -> 16.1 us
    all_to_all x2 -> x1, blocking collectives: 37.8 us -> 20 us  [local(): lax.all_to_all(up_half, 'fs', split_axis=0, concat_axis=1, tiled=True)]
    ppermute x0 -> x3, waiting for transfers between devices: none -> 12.9 us  [rotated_exchange(): lax.ppermute(sent, axis, [(i, (i + turn) % size) for i in range(size)])]
    ppermute x0 -> x3, starting transfers between devices: none -> 3.85 us  [rotated_exchange(): lax.ppermute(sent, axis, [(i, (i + turn) % size) for i in range(size)])]
  transfers between devices with their start and end apart: 5 -> 8, of which waited for: 4 -> 6; matrix products, arithmetic and copies ran while one was open for 3% -> 4% of each run, Pallas kernels for 0% -> 0%
where the time goes in v1:
time: 174 us; the launch traced here: 173 us
  waiting for transfers between devices  89.7 us (52%)
  blocking collectives  28.4 us (16%)
  starting transfers between devices  16.1 us (9%)
  between operations  14.3 us (8%)
  matrix products  12.3 us (7%)
  other arithmetic  6.49 us (4%)
  local copies, waits for them, and re-layouts  5.92 us (3%)
    reduce_scatter x1, waiting for transfers between devices, local(): lax.psum_scatter(products.reshape(local_width * lax.axis_size('tp'), shar...  35.3 us
    all_to_all x1, blocking collectives, local(): lax.all_to_all(up_half, 'fs', split_axis=0, concat_axis=1, tiled=True)  20 us
    all_to_all x1, waiting for transfers between devices, local(): lax.all_to_all(summed.reshape(local_width, shards, per_device * capacity)...  17.8 us
    all_to_all x1, waiting for transfers between devices, local(): lax.all_to_all(gate_half, 'fs', split_axis=0, concat_axis=1, tiled=True)  13.1 us
    ppermute x3, waiting for transfers between devices, rotated_exchange(): lax.ppermute(sent, axis, [(i, (i + turn) % size) for i in range(size)])  12.9 us
    all_to_all x1, waiting for transfers between devices, local(): lax.all_to_all(down_half, 'fs', split_axis=0, concat_axis=1, tiled=True)  10.5 us
    psum x1, blocking collectives, local(): squares = lax.psum(jnp.sum(local_values * local_values, axis=1), 'tp')  8.37 us
    dot_general x1, matrix products, local(): jnp.einsum('xdf,xscf->dsxc', down_serve, hidden, preferred_element_type=j...  5.81 us
  transfers between devices with their start and end apart: 8, of which 6 were waited for; matrix products, arithmetic and copies ran while one was open for 4% of the time, Pallas kernels for 0%

profile of v1, /device:TPU:0, one launch (start us, length us, event | category | flops | bytes accessed | tf_op | source)
XLA Modules:
  0.0 173.2 jit_solution(6029193446460293392)
XLA Ops:
  7.2 0.9 copy.17
  8.3 1.2 reduce-window.6
  11.0 1.1 fusion.8
  12.0 8.4 %psum.7 = f32[224]{0:T(256)S(1)} all-reduce(f32[224]{0:T(256)S(1)} %fusion.8), channel_id=1, replica_groups=mesh['grp'=2,'fs'=4,'tp'=4] {'tp'}, use_global_device_ids=true, to_apply=%region_4.5 | all-reduce | flops 224 | bytes 1792 | tf_op jit(solution)/shard_map/psum | solution.py:69
  20.4 1.5 convolution_convert_fusion.1
  21.9 1.6 collective-permute-start
  23.6 5.6 %collective-permute-done = bf16[1,1,168,512]{3,2,0,1:T(8,128)(2,1)S(1)} collective-permute-done((bf16[1,1,168,512]{3,2,0,1:T(8,128)(2,1)S(1)}, bf16[1,1,168,512]{3,2,0,1:T(8,128)(2,1)S(1)}, u32[]{:S(2)}, u32[]{:S(2)}) %collective-permute-start) | collective-permute-done | bytes 172064 | tf_op jit(solution)/shard_map/ppermute | solution.py:27
  29.2 0.9 collective-permute-start.1
  30.1 1.3 collective-permute-start.2
  31.5 7.3 %collective-permute-done.1 = bf16[1,1,168,512]{3,2,0,1:T(8,128)(2,1)S(1)} collective-permute-done((bf16[1,1,168,512]{3,2,0,1:T(8,128)(2,1)S(1)}, bf16[1,1,168,512]{3,2,0,1:T(8,128)(2,1)S(1)}, u32[]{:S(2)}, u32[]{:S(2)}) %collective-permute-start.1) | collective-permute-done | bytes 172064 | tf_op jit(solution)/shard_map/ppermute | solution.py:27
  39.7 2.3 %multiply_convert_fusion = (bf16[4,512,128]{2,1,0:T(8,128)(2,1)S(1)}, bf16[4,512,128]{2,1,0:T(8,128)(2,1)}) fusion(f32[4,512,128]{2,1,0:T(8,128)S(1)} %copy-done.5, f32[512]{0:T(512)S(1)} %copy-done.7, f32[4,512,128]{2,1,0:T(8,128)} %param.11), kind=kLoop, calls=%fused_computation.10 | loop fusion | flops 1048576 | bytes 3147776 | tf_op jit(solution)/shard_map/convert_element_type | solution.py:52
  42.1 20.0 %all_to_all.41 = bf16[4,512,128]{2,1,0:T(8,128)(2,1)S(1)} all-to-all(bf16[4,512,128]{2,1,0:T(8,128)(2,1)S(1)} %get-tuple-element.11), channel_id=1, replica_groups=mesh['grp'=2,'fs'=4,'tp'=4] {'fs'}, dimensions={0} | all-to-all | bytes 1048576 | tf_op jit(solution)/shard_map/all_to_all | solution.py:56
  62.1 3.5 %all-to-all-start = ((bf16[4,512,128]{2,1,0:T(8,128)(2,1)}), bf16[4,512,128]{2,1,0:T(8,128)(2,1)S(1)}, u32[]{:S(2)}, u32[]{:S(2)}) async-start(bf16[4,512,128]{2,1,0:T(8,128)(2,1)} %get-tuple-element.12), calls=%async_computation | async-start | bytes 1048576 | tf_op jit(solution)/shard_map/all_to_all | solution.py:55
  65.6 0.9 convert_element_type.49
  66.4 13.1 %all-to-all-done = bf16[4,512,128]{2,1,0:T(8,128)(2,1)S(1)} async-done(((bf16[4,512,128]{2,1,0:T(8,128)(2,1)}), bf16[4,512,128]{2,1,0:T(8,128)(2,1)S(1)}, u32[]{:S(2)}, u32[]{:S(2)}) %all-to-all-start) | async-done | bytes 524320 | tf_op jit(solution)/shard_map/all_to_all | solution.py:55
  79.6 4.1 %all-to-all-start.2 = ((bf16[4,512,128]{2,1,0:T(8,128)(2,1)}), bf16[4,512,128]{2,1,0:T(8,128)(2,1)}, u32[]{:S(2)}, u32[]{:S(2)}) async-start(bf16[4,512,128]{2,1,0:T(8,128)(2,1)} %convert_element_type.49), calls=%async_computation.2 | async-start | bytes 1048576 | tf_op jit(solution)/shard_map/all_to_all | solution.py:57
  83.8 3.5 %fusion = f32[4,168,128]{2,1,0:T(8,128)} fusion(bf16[2048,128,1]{1,0,2:T(8,128)(2,1)S(1)} %bitcast.48, bf16[4,1,168,2048]{3,2,0,1:T(8,128)(2,1)} %all-gather.2.cloned.1.call-done), kind=kOutput, calls=%fused_computation.1 | convolution fusion | flops 352321536 | bytes 3620864 | tf_op jit(solution)/shard_map/sxcd,xdf->xscf/dot_general | solution.py:83
  87.4 10.5 %all-to-all-done.2 = bf16[4,512,128]{2,1,0:T(8,128)(2,1)} async-done(((bf16[4,512,128]{2,1,0:T(8,128)(2,1)}), bf16[4,512,128]{2,1,0:T(8,128)(2,1)}, u32[]{:S(2)}, u32[]{:S(2)}) %all-to-all-start.2) | async-done | bytes 524320 | tf_op jit(solution)/shard_map/all_to_all | solution.py:57
  97.8 5.8 %convolution_convert_fusion = bf16[4,168,2048]{2,1,0:T(8,128)(2,1)} fusion(bf16[2048,128,1]{1,0,2:T(8,128)(2,1)} %bitcast.14, f32[4,168,128]{2,1,0:T(8,128)} %fusion, bf16[2048,128,1]{1,0,2:T(8,128)(2,1)} %bitcast.50, bf16[4,1,168,2048]{3,2,0,1:T(8,128)(2,1)S(1)} %copy-done), kind=kOutput, calls=%fused_computation | convolution fusion | flops 706535424 | bytes 6897664 | tf_op jit(solution)/shard_map/xdf,xscf->dsxc/dot_general | solution.py:87
  103.7 35.3 %reduce-scatter.2.cloned.1.call-done = bf16[512,672]{0,1:T(8,128)(2,1)} async-done(((bf16[2048,672]{0,1:T(8,128)(2,1)}), bf16[512,672]{0,1:T(8,128)(2,1)}) %reduce-scatter.2.cloned.1.call-update) | async-done | bytes 688144 | tf_op jit(solution)/shard_map/reduce_scatter | solution.py:88
  138.9 4.6 %all-to-all-start.3 = ((bf16[512,4,168]{0,2,1:T(8,128)(2,1)}), bf16[512,4,168]{0,2,1:T(8,128)(2,1)S(1)}, u32[]{:S(2)}, u32[]{:S(2)}) async-start(bf16[512,4,168]{0,2,1:T(8,128)(2,1)} %bitcast.56), calls=%async_computation.4 | async-start | bytes 1376256 | tf_op jit(solution)/shard_map/all_to_all | solution.py:96
  143.6 17.8 %all-to-all-done.3 = bf16[512,4,168]{0,2,1:T(8,128)(2,1)S(1)} async-done(((bf16[512,4,168]{0,2,1:T(8,128)(2,1)}), bf16[512,4,168]{0,2,1:T(8,128)(2,1)S(1)}, u32[]{:S(2)}, u32[]{:S(2)}) %all-to-all-start.3) | async-done | bytes 688160 | tf_op jit(solution)/shard_map/all_to_all | solution.py:96
  161.8 1.1 fusion.5
  164.5 1.9 %copy.30 = bf16[1,2048,128]{2,1,0:T(8,128)(2,1)} copy(bf16[1,2048,128]{2,1,0:T(8,128)(2,1)} %bitcast.2) | data formatting | bytes 1048576
  (44 shorter events, 4.7 us)
Async XLA Ops:
  7.2 32.5 %copy-start.7 = (f32[512]{0:T(512)S(1)}, f32[512]{0:T(512)}, u32[]{:S(2)}) copy-start(f32[512]{0:T(512)} %param.10) | copy-start | bytes 6148
  7.2 32.5 %copy-start.5 = (f32[4,512,128]{2,1,0:T(8,128)S(1)}, f32[4,512,128]{2,1,0:T(8,128)}, u32[]{:S(2)}) copy-start(f32[4,512,128]{2,1,0:T(8,128)} %param.12) | copy-start | bytes 3145732
  7.2 76.6 %all-gather.2.cloned.1.call-start = ((), (), s32[]{:S(2)}) async-start(), calls=%async_computation.5 | async-start | bytes 3440640 | tf_op jit(solution)/shard_map/all_gather | solution.py:79
  21.9 7.3 %collective-permute-start = (bf16[1,1,168,512]{3,2,0,1:T(8,128)(2,1)S(1)}, bf16[1,1,168,512]{3,2,0,1:T(8,128)(2,1)S(1)}, u32[]{:S(2)}, u32[]{:S(2)}) collective-permute-start(bf16[1,1,168,512]{3,2,0,1:T(8,128)(2,1)S(1)} %constant_dynamic-slice_fusion.2), channel_id=1, source_target_pairs={{0,4},{4,8},{8,12},{12,0},{1,5},{5,9},{9,13},{13,1},{2,6},{6,10},{... | collective-permute-start | bytes 516104 | tf_op jit(solution)/shard_map/ppermute | solution.py:27
  29.2 9.5 %collective-permute-start.1 = (bf16[1,1,168,512]{3,2,0,1:T(8,128)(2,1)S(1)}, bf16[1,1,168,512]{3,2,0,1:T(8,128)(2,1)S(1)}, u32[]{:S(2)}, u32[]{:S(2)}) collective-permute-start(bf16[1,1,168,512]{3,2,0,1:T(8,128)(2,1)S(1)} %get-tuple-element.5), channel_id=1, source_target_pairs={{0,8},{4,12},{8,0},{12,4},{1,9},{5,13},{9,1},{13,5},{2,10},{6,14},... | collective-permute-start | bytes 516104 | tf_op jit(solution)/shard_map/ppermute | solution.py:27
  30.1 8.7 %collective-permute-start.2 = (bf16[1,1,168,512]{3,2,0,1:T(8,128)(2,1)S(1)}, bf16[1,1,168,512]{3,2,0,1:T(8,128)(2,1)S(1)}, u32[]{:S(2)}, u32[]{:S(2)}) collective-permute-start(bf16[1,1,168,512]{3,2,0,1:T(8,128)(2,1)S(1)} %get-tuple-element.4), channel_id=1, source_target_pairs={{0,12},{4,0},{8,4},{12,8},{1,13},{5,1},{9,5},{13,9},{2,14},{6,2},{... | collective-permute-start | bytes 516104 | tf_op jit(solution)/shard_map/ppermute | solution.py:27
  38.8 0.8 copy-start.3
  39.7 25.8 %copy-start.4 = (f32[4,512,128]{2,1,0:T(8,128)S(1)}, f32[4,512,128]{2,1,0:T(8,128)}, u32[]{:S(2)}) copy-start(f32[4,512,128]{2,1,0:T(8,128)} %param.13) | copy-start | bytes 3145732
  62.1 17.5 %all-to-all-start = ((bf16[4,512,128]{2,1,0:T(8,128)(2,1)}), bf16[4,512,128]{2,1,0:T(8,128)(2,1)S(1)}, u32[]{:S(2)}, u32[]{:S(2)}) async-start(bf16[4,512,128]{2,1,0:T(8,128)(2,1)} %get-tuple-element.12), calls=%async_computation | async-start | bytes 1048576 | tf_op jit(solution)/shard_map/all_to_all | solution.py:55
  79.6 4.2 %copy-start.1 = (bf16[4,512,128]{2,1,0:T(8,128)(2,1)}, bf16[4,512,128]{2,1,0:T(8,128)(2,1)S(1)}, u32[]{:S(2)}) copy-start(bf16[4,512,128]{2,1,0:T(8,128)(2,1)S(1)} %all-to-all-done) | copy-start | bytes 1572868
  79.6 18.3 %all-to-all-start.2 = ((bf16[4,512,128]{2,1,0:T(8,128)(2,1)}), bf16[4,512,128]{2,1,0:T(8,128)(2,1)}, u32[]{:S(2)}, u32[]{:S(2)}) async-start(bf16[4,512,128]{2,1,0:T(8,128)(2,1)} %convert_element_type.49), calls=%async_computation.2 | async-start | bytes 1048576 | tf_op jit(solution)/shard_map/all_to_all | solution.py:57
  83.7 55.2 %reduce-scatter.2.cloned.1.call-start = ((), (), s32[]{:S(2)}) async-start(), calls=%async_computation.6 | async-start | bytes 3440640 | tf_op jit(solution)/shard_map/reduce_scatter | solution.py:88
  83.8 14.0 %copy-start = (bf16[4,1,168,2048]{3,2,0,1:T(8,128)(2,1)S(1)}, bf16[4,1,168,2048]{3,2,0,1:T(8,128)(2,1)}, u32[]{:S(2)}) copy-start(bf16[4,1,168,2048]{3,2,0,1:T(8,128)(2,1)} %all-gather.2.cloned.1.call-done) | copy-start | bytes 8257540
  103.7 39.9 %copy-start.6 = (f32[224,2]{0,1:T(2,128)S(1)}, f32[224,2]{0,1:T(2,128)}, u32[]{:S(2)}) copy-start(f32[224,2]{0,1:T(2,128)} %param.9) | copy-start | bytes 5380
  103.7 59.2 %copy-start.2 = (bf16[4,512,128]{2,1,0:T(8,128)(2,1)S(1)}, bf16[4,512,128]{2,1,0:T(8,128)(2,1)}, u32[]{:S(2)}) copy-start(bf16[4,512,128]{2,1,0:T(8,128)(2,1)} %copy-done.1) | copy-start | bytes 1572868
  138.9 22.4 %all-to-all-start.3 = ((bf16[512,4,168]{0,2,1:T(8,128)(2,1)}), bf16[512,4,168]{0,2,1:T(8,128)(2,1)S(1)}, u32[]{:S(2)}, u32[]{:S(2)}) async-start(bf16[512,4,168]{0,2,1:T(8,128)(2,1)} %bitcast.56), calls=%async_computation.4 | async-start | bytes 1376256 | tf_op jit(solution)/shard_map/all_to_all | solution.py:96
Sparse Core Ops, SparseCore 0:
  39.8 29.0 all-gather.1
  103.8 35.1 reduce-scatter.1
